TPU v7x, 256 devices: a whole 4x4x8 slice. The times are simulated.
256 devices in a mesh: sp: 64 (over z, x, core), tp: 4 (over y).
Axes of the slice: x: 4, y: 4, z: 8, core: 2. Of those that a mesh axis runs over, the one named last changes fastest.
Arguments:
- queries: bfloat16 [32768, 2048], P('sp', 'tp'), may hold values from -90 to 90, as said below
- key_rows: bfloat16 [32768, 512], P('sp', 'tp'), may hold values from -6 to 6
- value_rows: bfloat16 [32768, 512], P('sp', 'tp'), may hold values from -6 to 6
- sink_logits: float32 [16], P('tp'), may hold values from 2 to 7
- residual: bfloat16 [32768, 2048], P('sp'), may hold values from -6 to 6
- norm_gain: float32 [2048], replicated, may hold values from 0.1 to 1.9
- out_weight: bfloat16 [2048, 2048], P('tp'), may hold values from -1.5 to 1.5
- gate_weight: bfloat16 [2048, 5632], P('sp', 'tp'), may hold values from -0.125 to 0.125
- up_weight: bfloat16 [2048, 5632], P('sp', 'tp'), may hold values from -0.125 to 0.125
- down_weight: bfloat16 [5632, 2048], P('tp', 'sp'), may hold values from -0.078125 to 0.078125
Outputs:
- mixed: bfloat16 [32768, 2048], P(('sp', 'tp'))
Inputs may be any that keep to these rules, and one draw needn't show every extreme that they name: queries are mostly of order one; some rows may be much larger.
All inputs are finite; a program needn't handle non-finite values.
Results may differ from a plain program's by a relative error of at most 0.012.
Values may be sent and summed in bfloat16 or wider, within the bound.
A program may use at most 128 MiB of HBM per device.

v0:
```python
import jax
import jax.numpy as jnp
from jax import lax
from jax.sharding import PartitionSpec as P

DH = 128
WIN = 128
EPSILON = 1e-06
MASKED = -1e30


def with_halo(cells, sides, width):
    for axis, dim in sides:
        count = lax.axis_size(axis)
        ends = count - 1
        head = lax.slice_in_dim(cells, 0, width, axis=dim)
        tail = lax.slice_in_dim(cells, cells.shape[dim] - width, cells.shape[dim], axis=dim)
        cells = jnp.concatenate(
            [
                lax.ppermute(tail, axis, [(i, (i + 1) % count) for i in range(ends)]),
                cells,
                lax.ppermute(head, axis, [((i + 1) % count, i) for i in range(ends)]),
            ],
            axis=dim,
        )
    return cells


def split_up(value, dim, size):
    before, after = (value.shape[:dim], value.shape[dim + 1 :])
    return jnp.moveaxis(value.reshape(*before, size, -1, *after), dim, 0)


def sent_and_summed(value, axis, dim):
    size = lax.axis_size(axis)
    blocks = lax.all_to_all(split_up(value, dim, size), axis, 0, 0, tiled=True)
    return jnp.sum(blocks.astype(jnp.float32), axis=0)


def sent_to_all(value, axis):
    size = lax.axis_size(axis)
    return lax.all_to_all(
        jnp.broadcast_to(value[None], (size, *value.shape)), axis, 0, 0, tiled=True
    )


def laid_out(blocks, dim):
    blocks = jnp.moveaxis(blocks, 0, dim)
    lengths = blocks.shape
    return blocks.reshape(*lengths[:dim], lengths[dim] * lengths[dim + 1], *lengths[dim + 2 :])


def gather_directly(value, axis, dim):
    blocks = sent_to_all(value, axis)
    return laid_out(blocks, dim)


def side_by_side(arrays, axis, dim, along):
    ends, at = ([], 0)
    for a in arrays[:-1]:
        at += a.shape[along]
        ends.append(at)
    both = jnp.concatenate(arrays, axis=along)
    return tuple(jnp.split(lax.all_gather(both, axis, axis=dim, tiled=True), ends, axis=along))


def attend_block(query_blk, key_blk, value_blk, sink_logits, query_pos, key_pos, seq_len):
    kv_heads = key_blk.shape[1] // DH
    group_size = query_blk.shape[1] // key_blk.shape[1]
    query_four = query_blk.reshape(query_blk.shape[0], kv_heads, group_size, DH)
    key_three = key_blk.reshape(key_blk.shape[0], kv_heads, DH)
    value_three = value_blk.reshape(value_blk.shape[0], kv_heads, DH)
    scores = jnp.einsum(
        "qhgd,khd->hgqk", query_four, key_three, preferred_element_type=jnp.float32
    ) * DH ** (-0.5)
    allowed = (
        (jnp.abs(key_pos[None, :] - query_pos[:, None]) <= WIN)
        & (key_pos[None, :] >= 0)
        & (key_pos[None, :] < seq_len)
    )
    scores = jnp.where(allowed[None, None], scores, MASKED)
    sink_col = sink_logits.reshape(kv_heads, group_size)[:, :, None]
    highest = jnp.maximum(jnp.max(scores, axis=-1), sink_col)
    weights_exp = jnp.exp(scores - highest[..., None])
    denominator = jnp.sum(weights_exp, axis=-1) + jnp.exp(sink_col - highest)
    probabilities = (weights_exp / denominator[..., None]).astype(jnp.bfloat16)
    heads_out = jnp.einsum(
        "hgqk,khd->qhgd", probabilities, value_three, preferred_element_type=jnp.float32
    )
    return heads_out.astype(jnp.bfloat16).reshape(query_blk.shape[0], kv_heads * group_size * DH)


def rms_scale(rows_wide, norm_gain):
    mean_square = jnp.mean(rows_wide * rows_wide, axis=-1, keepdims=True)
    return (rows_wide * lax.rsqrt(mean_square + EPSILON) * norm_gain).astype(jnp.bfloat16)


def fetch_down(down_weight):
    return lax.all_gather(down_weight, "sp", axis=1, tiled=True)


def shards(
    queries,
    key_rows,
    value_rows,
    sink_logits,
    residual,
    norm_gain,
    out_weight,
    gate_weight,
    up_weight,
    down_weight,
):
    tok_local = queries.shape[0]
    block_len = 2 * WIN
    share_rows = tok_local // lax.axis_size("tp")
    seq_len = tok_local * lax.axis_size("sp")
    device_offset = lax.axis_index("sp") * tok_local
    kv_pair = jnp.stack([key_rows, value_rows])
    kv_ext = with_halo(kv_pair, (("sp", 1),), WIN)

    def one_block(block_index):
        block_first = block_index * block_len
        query_blk = lax.dynamic_slice_in_dim(queries, block_first, block_len, 0)
        key_blk = lax.dynamic_slice_in_dim(kv_ext[0], block_first, block_len + 2 * WIN, 0)
        value_blk = lax.dynamic_slice_in_dim(kv_ext[1], block_first, block_len + 2 * WIN, 0)
        query_pos = device_offset + block_first + jnp.arange(block_len, dtype=jnp.int32)
        key_pos = (
            device_offset + block_first - WIN + jnp.arange(block_len + 2 * WIN, dtype=jnp.int32)
        )
        return attend_block(query_blk, key_blk, value_blk, sink_logits, query_pos, key_pos, seq_len)

    blocks = lax.map(one_block, jnp.arange(tok_local // block_len, dtype=jnp.int32))
    attended = blocks.reshape(tok_local, queries.shape[1])
    own_first = lax.axis_index("tp") * share_rows
    picked = attended
    attn_share = sent_and_summed(
        jnp.dot(picked, out_weight, preferred_element_type=jnp.float32).astype(jnp.bfloat16),
        "tp",
        0,
    )
    middle_own = (
        lax.dynamic_slice_in_dim(residual, own_first, share_rows, 0).astype(jnp.float32)
        + attn_share
    )
    normed_all = gather_directly(rms_scale(middle_own, norm_gain), "tp", 0)
    pieces = side_by_side((gate_weight, up_weight), "sp", 0, 1)
    gate_sectioned = pieces[0]
    up_sectioned = pieces[1]
    gate_acc = jnp.dot(normed_all, gate_sectioned, preferred_element_type=jnp.float32)
    up_acc = jnp.dot(normed_all, up_sectioned, preferred_element_type=jnp.float32)
    down_whole = fetch_down(down_weight)
    hidden = (jax.nn.silu(gate_acc) * up_acc).astype(jnp.bfloat16)
    picked = hidden
    ffn_share = lax.psum_scatter(
        jnp.dot(picked, down_whole, preferred_element_type=jnp.float32).astype(jnp.bfloat16),
        "tp",
        scatter_dimension=0,
        tiled=True,
    ).astype(jnp.float32)
    return (middle_own + ffn_share).astype(jnp.bfloat16)


def solution(mesh):
    placed = (
        P("sp", "tp"),
        P("sp", "tp"),
        P("sp", "tp"),
        P("tp"),
        P("sp", None),
        P(),
        P("tp", None),
        P("sp", "tp"),
        P("sp", "tp"),
        P("tp", "sp"),
    )
    return jax.shard_map(
        shards, mesh=mesh, in_specs=placed, out_specs=P(("sp", "tp"), None), check_vma=False
    )
```

profile of v0, /device:TPU:1, one launch (start us, length us, event | category | flops | bytes accessed | tf_op | source)
XLA Modules:
  0.0 233.1 jit_solution(577112236005821725)
XLA Ops:
  6.5 1.8 pad_maximum_fusion.1
  8.3 0.0 all-gather.5.cloned.1.call-start
  8.4 0.7 all-gather.5.cloned.1.call-update
  9.1 0.8 pad_maximum_fusion.3
  9.9 4.5 %collective-permute-start = (bf16[2,128,128]{2,1,0:T(8,128)(2,1)S(1)}, bf16[2,128,128]{2,1,0:T(8,128)(2,1)S(1)}, u32[]{:S(2)}, u32[]{:S(2)}) collective-permute-start(bf16[2,128,128]{2,1,0:T(8,128)(2,1)S(1)} %get-tuple-element.122), channel_id=1, source_target_pairs={{0,4},{4,8},{8,12},{12,16},{16,20},{20,24},{24,28},{28,32},{32,36}... | collective-permute-start | bytes 196616 | tf_op jit(solution)/shard_map/ppermute | solution.py:20
  14.4 1.9 collective-permute-start.1
  16.4 3.6 %collective-permute-done.1 = bf16[2,128,128]{2,1,0:T(8,128)(2,1)S(1)} collective-permute-done((bf16[2,128,128]{2,1,0:T(8,128)(2,1)S(1)}, bf16[2,128,128]{2,1,0:T(8,128)(2,1)S(1)}, u32[]{:S(2)}, u32[]{:S(2)}) %collective-permute-start.1) | collective-permute-done | bytes 65568 | tf_op jit(solution)/shard_map/ppermute | solution.py:22
  20.0 1.0 pad_maximum_fusion
  21.0 11.1 %while.12 = (s32[]{:T(128)}, bf16[2,256,512]{2,1,0:T(8,128)(2,1)}, bf16[2,768,128]{2,1,0:T(8,128)(2,1)S(1)}, s32[2]{0:T(128)S(1)}, s32[]{:T(128)}, /*index=5*/bf...) while((s32[]{:T(128)}, bf16[2,256,512]{2,1,0:T(8,128)(2,1)}, ...), condition=%wide.region_3.4_spmd, body=%wide.region_0.3_spmd.sunk | while | flops 273420544 | bytes 14467520 | solution.py:133
  21.0 0.6 dynamic_slice.48
  22.3 0.3 fusion.46
  22.6 1.0 constant_dynamic-slice_fusion.2
  23.6 0.1 copy.25
  23.7 0.5 fusion.47
  24.2 0.1 broadcast_maximum_fusion.2
  24.3 0.3 fusion.48
  24.6 0.1 exponential_add_fusion.2
  24.7 0.5 convolution_convert_fusion.4
  25.2 0.1 copy.26
  25.4 0.4 copy-done.4
  25.8 0.8 copy-done.5
  26.6 0.6 dynamic_slice.48
  27.8 0.3 fusion.46
  28.1 1.0 constant_dynamic-slice_fusion.2
  29.1 0.1 copy.25
  29.3 0.5 fusion.47
  29.8 0.1 broadcast_maximum_fusion.2
  29.8 0.3 fusion.48
  30.1 0.1 exponential_add_fusion.2
  30.2 0.5 convolution_convert_fusion.4
  30.8 0.1 copy.26
  30.9 0.4 copy-done.4
  31.3 0.8 copy-done.5
  32.1 3.6 %convolution_convert_fusion.1 = bf16[512,2048]{1,0:T(8,128)(2,1)} fusion(bf16[512,512]{1,0:T(8,128)(2,1)} %bitcast.59, bf16[512,2048]{1,0:T(8,128)(2,1)S(1)} %copy-done), kind=kOutput, calls=%fused_computation.30 | convolution fusion | flops 1074790400 | bytes 4718592 | tf_op jit(solution)/shard_map/dot_general | solution.py:138
  35.7 4.4 %all-to-all-start = ((bf16[4,128,2048]{2,1,0:T(8,128)(2,1)}), bf16[4,128,2048]{2,1,0:T(8,128)(2,1)}, u32[]{:S(2)}, u32[]{:S(2)}) async-start(bf16[4,128,2048]{2,1,0:T(8,128)(2,1)} %bitcast.52), calls=%async_computation | async-start | bytes 4194304 | tf_op jit(solution)/shard_map/all_to_all | solution.py:36
  40.2 0.0 reduce-scatter.2.cloned.1.call-start
  40.2 24.7 %all-to-all-done = bf16[4,128,2048]{2,1,0:T(8,128)(2,1)} async-done(((bf16[4,128,2048]{2,1,0:T(8,128)(2,1)}), bf16[4,128,2048]{2,1,0:T(8,128)(2,1)}, u32[]{:S(2)}, u32[]{:S(2)}) %all-to-all-start) | async-done | bytes 2097184 | tf_op jit(solution)/shard_map/all_to_all | solution.py:36
  64.9 2.2 convert_reduce_fusion
  67.2 0.2 multiply_reduce_fusion
  67.4 0.2 multiply_convert_fusion
  67.6 0.2 broadcast_in_dim.44
  67.9 30.0 %all_to_all.10 = bf16[4,128,2048]{2,1,0:T(8,128)(2,1)} all-to-all(bf16[4,128,2048]{2,1,0:T(8,128)(2,1)S(1)} %broadcast_in_dim.44), channel_id=1, replica_groups=mesh['sp'=64,'tp'=4] {'tp'}, dimensions={0} | all-to-all | bytes 4194304 | tf_op jit(solution)/shard_map/all_to_all | solution.py:42
  97.9 4.1 %all-gather.3.cloned.1.call-done = bf16[2048,2816]{1,0:T(8,128)(2,1)} async-done(((bf16[32,2816]{1,0:T(8,128)(2,1)}), bf16[2048,2816]{1,0:T(8,128)(2,1)}) %all-gather.3.cloned.1.call-update) | async-done | bytes 11534352 | tf_op jit(solution)/shard_map/all_gather | solution.py:64
  102.0 8.2 %fusion.14 = f32[512,1408]{1,0:T(8,128)} fusion(bf16[512,2048]{1,0:T(8,128)(2,1)} %bitcast.53, bf16[2048,2816]{1,0:T(8,128)(2,1)} %all-gather.3.cloned.1.call-done), kind=kOutput, calls=%fused_computation.25 | convolution fusion | flops 2952790016 | bytes 10747904 | tf_op jit(solution)/shard_map/dot_general | solution.py:150
  110.2 71.3 %all-gather.5.cloned.1.call-done = bf16[1408,2048]{0,1:T(8,128)(2,1)} async-done(((bf16[1408,32]{0,1:T(8,128)(2,1)}), bf16[1408,2048]{0,1:T(8,128)(2,1)}) %all-gather.5.cloned.1.call-update) | async-done | bytes 5767184 | tf_op jit(solution)/shard_map/all_gather | solution.py:99
  181.5 13.8 %convolution_convert_fusion.2 = bf16[512,2048]{1,0:T(8,128)(2,1)} fusion(bf16[1408,2048]{0,1:T(8,128)(2,1)} %all-gather.5.cloned.1.call-done, bf16[512,2048]{1,0:T(8,128)(2,1)} %bitcast.54, bf16[2048,2816]{1,0:T(8,128)(2,1)} %all-gather.3.cloned.1.call-done, f32[512,1408]{1,0:T(8,128)} %fusion.14), kind=kOutput, calls=%fused_computation.31 | convolution fusion | flops 5910953984 | bytes 18612224 | tf_op jit(solution)/shard_map/dot_general | solution.py:156
  195.4 29.0 %reduce-scatter.2.cloned.1.call-done = bf16[128,2048]{1,0:T(8,128)(2,1)} async-done(((bf16[512,2048]{1,0:T(8,128)(2,1)}), bf16[128,2048]{1,0:T(8,128)(2,1)}) %reduce-scatter.2.cloned.1.call-update) | async-done | bytes 524304 | tf_op jit(solution)/shard_map/reduce_scatter | solution.py:155
  224.4 2.2 add_convert_fusion
  (31 shorter events, 0.2 us)
Async XLA Ops:
  6.5 25.6 %copy-start = (bf16[512,2048]{1,0:T(8,128)(2,1)S(1)}, bf16[512,2048]{1,0:T(8,128)(2,1)}, u32[]{:S(2)}) copy-start(bf16[512,2048]{1,0:T(8,128)(2,1)} %param.18) | copy-start | bytes 6291460
  6.5 95.5 %all-gather.3.cloned.1.call-start = ((), (), s32[]{:S(2)}) async-start(), calls=%async_computation.3 | async-start | bytes 11714560 | tf_op jit(solution)/shard_map/all_gather | solution.py:64
  8.3 173.2 %all-gather.5.cloned.1.call-start = ((), (), s32[]{:S(2)}) async-start(), calls=%async_computation.4 | async-start | bytes 5857280 | tf_op jit(solution)/shard_map/all_gather | solution.py:99
  9.9 6.5 %collective-permute-start = (bf16[2,128,128]{2,1,0:T(8,128)(2,1)S(1)}, bf16[2,128,128]{2,1,0:T(8,128)(2,1)S(1)}, u32[]{:S(2)}, u32[]{:S(2)}) collective-permute-start(bf16[2,128,128]{2,1,0:T(8,128)(2,1)S(1)} %get-tuple-element.122), channel_id=1, source_target_pairs={{0,4},{4,8},{8,12},{12,16},{16,20},{20,24},{24,28},{28,32},{32,36}... | collective-permute-start | bytes 196616 | tf_op jit(solution)/shard_map/ppermute | solution.py:20
  14.4 5.6 %collective-permute-start.1 = (bf16[2,128,128]{2,1,0:T(8,128)(2,1)S(1)}, bf16[2,128,128]{2,1,0:T(8,128)(2,1)S(1)}, u32[]{:S(2)}, u32[]{:S(2)}) collective-permute-start(bf16[2,128,128]{2,1,0:T(8,128)(2,1)S(1)} %get-tuple-element.123), channel_id=1, source_target_pairs={{4,0},{8,4},{12,8},{16,12},{20,16},{24,20},{28,24},{32,28},{36,32}... | collective-permute-start | bytes 196616 | tf_op jit(solution)/shard_map/ppermute | solution.py:22
  23.6 0.7 copy-start.2
  24.7 1.0 copy-start.4
  25.8 0.8 copy-start.5
  29.1 0.7 copy-start.2
  30.2 1.0 copy-start.4
  31.3 0.8 copy-start.5
  35.7 29.2 %all-to-all-start = ((bf16[4,128,2048]{2,1,0:T(8,128)(2,1)}), bf16[4,128,2048]{2,1,0:T(8,128)(2,1)}, u32[]{:S(2)}, u32[]{:S(2)}) async-start(bf16[4,128,2048]{2,1,0:T(8,128)(2,1)} %bitcast.52), calls=%async_computation | async-start | bytes 4194304 | tf_op jit(solution)/shard_map/all_to_all | solution.py:36
  40.2 184.2 %reduce-scatter.2.cloned.1.call-start = ((), (), s32[]{:S(2)}) async-start(), calls=%async_computation.5 | async-start | bytes 2621440 | tf_op jit(solution)/shard_map/reduce_scatter | solution.py:155
  40.2 27.2 %copy-start.3 = (f32[2048]{0:T(1024)S(1)}, f32[2048]{0:T(1024)}, u32[]{:S(2)}) copy-start(f32[2048]{0:T(1024)} %param.17) | copy-start | bytes 24580
  64.9 2.2 copy-start.1
Sparse Core Ops, SparseCore 0:
  10.1 91.8 all-gather.2
  104.7 76.7 all-gather.4
  195.5 28.8 reduce-scatter.1
where the time goes:
time: 234 us; the launch traced here: 233 us
  waiting for transfers between devices  133 us (57%)
  blocking collectives  30 us (13%)
  matrix products  27.7 us (12%)
  between operations  13.2 us (6%)
  starting transfers between devices  10.9 us (5%)
  other arithmetic  9.91 us (4%)
  local copies, waits for them, and re-layouts  6.4 us (3%)
    all_gather x1, waiting for transfers between devices, fetch_down(): return lax.all_gather(down_weight, 'sp', axis=1, tiled=True)  71.3 us
    all_to_all x1, blocking collectives, sent_to_all(): lax.all_to_all(jnp.broadcast_to(value[None], (size, *value.shape)), axis,...  30 us
    reduce_scatter x1, waiting for transfers between devices, shards(): lax.psum_scatter(jnp.dot(picked, down_whole, preferred_element_type=jnp.f...  29 us
    all_to_all x1, waiting for transfers between devices, sent_and_summed(): blocks = lax.all_to_all(split_up(value, dim, size), axis, 0, 0, tiled=True)  24.7 us
    dot_general x1, matrix products, shards(): jnp.dot(picked, down_whole, preferred_element_type=jnp.float32)  13.8 us
    dot_general x1, matrix products, shards(): jnp.dot(normed_all, gate_sectioned, preferred_element_type=jnp.float32)  8.23 us
  transfers between devices with their start and end apart: 6, of which 5 were waited for; matrix products, arithmetic and copies ran while one was open for 10% of the time, Pallas kernels for 0%

commit v1 on v0

--- a/solution.py
+++ b/solution.py
@@ -96,7 +96,14 @@
 
 
 def fetch_down(down_weight):
-    return lax.all_gather(down_weight, "sp", axis=1, tiled=True)
+
+    def pair_sectors(payload):
+        e_next = tuple((payload for _ in range(lax.axis_size("sp"))))
+        front = jnp.stack(e_next)
+        later = lax.all_to_all(front, "sp", 0, 0)
+        return jnp.concatenate(later, axis=1)
+
+    return pair_sectors(down_weight)
 
 
 def shards(

time: 234 us -> 293 us (1.25)
  waiting for transfers between devices: 133 us -> 176 us
  starting transfers between devices: 10.9 us -> 26.7 us
    all_to_all x0 -> x1, waiting for transfers between devices: none -> 119 us  [pair_sectors(): later = lax.all_to_all(front, 'sp', 0, 0)]
    all_gather x1 -> x0, waiting for transfers between devices: 71.3 us -> none  [fetch_down(): return lax.all_gather(down_weight, 'sp', axis=1, tiled=True)]
    all_to_all x0 -> x1, starting transfers between devices: none -> 15 us  [pair_sectors(): later = lax.all_to_all(front, 'sp', 0, 0)]
    all_gather x1, waiting for transfers between devices: 4.12 us -> 0.02 us  [side_by_side(): lax.all_gather(both, axis, axis=dim, tiled=True)]
    ppermute x1, waiting for transfers between devices: 3.63 us -> 0.01 us  [with_halo(): lax.ppermute(head, axis, [((i + 1) % count, i) for i in range(ends)])]
    ppermute x1, starting transfers between devices: 1.92 us -> 5.11 us  [with_halo(): lax.ppermute(head, axis, [((i + 1) % count, i) for i in range(ends)])]
  transfers between devices with their start and end apart: 6 -> 6, of which waited for: 5 -> 4; matrix products, arithmetic and copies ran while one was open for 10% -> 10% of each run, Pallas kernels for 0% -> 0%
where the time goes in v1:
time: 293 us
  waiting for transfers between devices  176 us (60%)
  blocking collectives  28.7 us (10%)
  matrix products  27.8 us (9%)
  starting transfers between devices  26.7 us (9%)
  between operations  13.5 us (5%)
  other arithmetic  10.2 us (3%)
  local copies, waits for them, and re-layouts  8.63 us (3%)
    all_to_all x1, waiting for transfers between devices, pair_sectors(): later = lax.all_to_all(front, 'sp', 0, 0)  119 us
    all_to_all x1, blocking collectives, sent_to_all(): lax.all_to_all(jnp.broadcast_to(value[None], (size, *value.shape)), axis,...  28.7 us
    reduce_scatter x1, waiting for transfers between devices, shards(): lax.psum_scatter(jnp.dot(picked, down_whole, preferred_element_type=jnp.f...  28.7 us
    all_to_all x1, waiting for transfers between devices, sent_and_summed(): blocks = lax.all_to_all(split_up(value, dim, size), axis, 0, 0, tiled=True)  26.4 us
    all_to_all x1, starting transfers between devices, pair_sectors(): later = lax.all_to_all(front, 'sp', 0, 0)  15 us
    dot_general x1, matrix products, shards(): jnp.dot(picked, down_whole, preferred_element_type=jnp.float32)  13.8 us
    dot_general x1, matrix products, shards(): jnp.dot(normed_all, gate_sectioned, preferred_element_type=jnp.float32)  8.3 us
  transfers between devices with their start and end apart: 6, of which 4 were waited for; matrix products, arithmetic and copies ran while one was open for 10% of the time, Pallas kernels for 0%

profile of v1, /device:TPU:1, one launch (start us, length us, event | category | flops | bytes accessed | tf_op | source)
XLA Modules:
  0.0 292.9 jit_solution(17788284408751387814)
XLA Ops:
  6.5 1.8 pad_maximum_fusion.1
  8.3 0.0 all-gather.2.cloned.1.call-update
  8.3 0.8 pad_maximum_fusion.3
  9.2 5.1 %collective-permute-start.1 = (bf16[2,128,128]{2,1,0:T(8,128)(2,1)S(1)}, bf16[2,128,128]{2,1,0:T(8,128)(2,1)S(1)}, u32[]{:S(2)}, u32[]{:S(2)}) collective-permute-start(bf16[2,128,128]{2,1,0:T(8,128)(2,1)S(1)} %get-tuple-element.123), channel_id=1, source_target_pairs={{4,0},{8,4},{12,8},{16,12},{20,16},{24,20},{28,24},{32,28},{36,32}... | collective-permute-start | bytes 196616 | tf_op jit(solution)/shard_map/ppermute | solution.py:22
  14.3 1.9 collective-permute-start
  16.2 1.3 collective-permute-done
  17.5 1.0 pad_maximum_fusion
  18.5 10.5 %while.12 = (s32[]{:T(128)}, bf16[2,256,512]{2,1,0:T(8,128)(2,1)}, bf16[2,768,128]{2,1,0:T(8,128)(2,1)S(1)}, s32[2]{0:T(128)S(1)}, s32[]{:T(128)}, /*index=5*/bf...) while((s32[]{:T(128)}, bf16[2,256,512]{2,1,0:T(8,128)(2,1)}, ...), condition=%wide.region_3.4_spmd, body=%wide.region_0.3_spmd.sunk | while | flops 273420544 | bytes 10273160 | solution.py:140
  18.5 0.7 dynamic_slice.48
  19.9 1.0 constant_dynamic-slice_fusion.2
  20.9 0.1 copy.26
  21.1 0.3 fusion.46
  21.4 0.5 fusion.47
  21.9 0.1 broadcast_maximum_fusion.2
  22.0 0.3 fusion.48
  22.3 0.1 exponential_add_fusion.2
  22.3 0.5 convolution_convert_fusion.4
  22.9 0.1 copy.27
  23.0 0.7 constant_dynamic-update-slice_fusion.2
  23.8 0.7 dynamic_slice.48
  25.1 1.0 constant_dynamic-slice_fusion.2
  26.1 0.1 copy.26
  26.4 0.3 fusion.46
  26.6 0.5 fusion.47
  27.1 0.1 broadcast_maximum_fusion.2
  27.2 0.3 fusion.48
  27.5 0.1 exponential_add_fusion.2
  27.6 0.5 convolution_convert_fusion.4
  28.1 0.1 copy.27
  28.3 0.7 constant_dynamic-update-slice_fusion.2
  29.0 3.6 %convolution_convert_fusion.1 = bf16[512,2048]{1,0:T(8,128)(2,1)} fusion(bf16[512,512]{1,0:T(8,128)(2,1)} %bitcast.62, bf16[512,2048]{1,0:T(8,128)(2,1)S(1)} %copy-done), kind=kOutput, calls=%fused_computation.30 | convolution fusion | flops 1074790400 | bytes 4718592 | tf_op jit(solution)/shard_map/dot_general | solution.py:145
  32.6 4.4 %all-to-all-start = ((bf16[4,128,2048]{2,1,0:T(8,128)(2,1)}), bf16[4,128,2048]{2,1,0:T(8,128)(2,1)}, u32[]{:S(2)}, u32[]{:S(2)}) async-start(bf16[4,128,2048]{2,1,0:T(8,128)(2,1)} %bitcast.55), calls=%async_computation | async-start | bytes 4194304 | tf_op jit(solution)/shard_map/all_to_all | solution.py:36
  37.1 26.4 %all-to-all-done = bf16[4,128,2048]{2,1,0:T(8,128)(2,1)} async-done(((bf16[4,128,2048]{2,1,0:T(8,128)(2,1)}), bf16[4,128,2048]{2,1,0:T(8,128)(2,1)}, u32[]{:S(2)}, u32[]{:S(2)}) %all-to-all-start) | async-done | bytes 2097184 | tf_op jit(solution)/shard_map/all_to_all | solution.py:36
  63.5 2.5 convert_reduce_fusion
  66.0 0.1 copy-done.1
  66.1 0.2 multiply_reduce_fusion
  66.3 0.2 multiply_convert_fusion
  66.6 0.2 broadcast_in_dim.44
  66.8 28.7 %all_to_all.15 = bf16[4,128,2048]{2,1,0:T(8,128)(2,1)} all-to-all(bf16[4,128,2048]{2,1,0:T(8,128)(2,1)S(1)} %broadcast_in_dim.44), channel_id=1, replica_groups=mesh['sp'=64,'tp'=4] {'tp'}, dimensions={0} | all-to-all | bytes 4194304 | tf_op jit(solution)/shard_map/all_to_all | solution.py:42
  95.6 2.9 stack.11
  98.5 15.0 %all-to-all-start.2 = ((bf16[64,1408,32]{1,2,0:T(8,128)(2,1)}), bf16[64,1408,32]{1,2,0:T(8,128)(2,1)}, u32[]{:S(2)}, u32[]{:S(2)}) async-start(bf16[64,1408,32]{1,2,0:T(8,128)(2,1)} %stack.11), calls=%async_computation.2 | async-start | bytes 11534336 | tf_op jit(solution)/shard_map/all_to_all | solution.py:103
  113.5 0.2 reduce-scatter.2.cloned.1.call-start
  113.7 0.0 all-gather.2.cloned.1.call-done
  113.7 8.3 %fusion.14 = f32[512,1408]{1,0:T(8,128)} fusion(bf16[512,2048]{1,0:T(8,128)(2,1)} %bitcast.56, bf16[2048,2816]{1,0:T(8,128)(2,1)} %all-gather.2.cloned.1.call-done), kind=kOutput, calls=%fused_computation.25 | convolution fusion | flops 2952790016 | bytes 10747904 | tf_op jit(solution)/shard_map/dot_general | solution.py:157
  122.0 119.2 %all-to-all-done.2 = bf16[64,1408,32]{1,2,0:T(8,128)(2,1)} async-done(((bf16[64,1408,32]{1,2,0:T(8,128)(2,1)}), bf16[64,1408,32]{1,2,0:T(8,128)(2,1)}, u32[]{:S(2)}, u32[]{:S(2)}) %all-to-all-start.2) | async-done | bytes 5767200 | tf_op jit(solution)/shard_map/all_to_all | solution.py:103
  241.2 13.8 %convolution_convert_fusion.2 = bf16[512,2048]{1,0:T(8,128)(2,1)} fusion(bf16[1408,2048]{0,1:T(8,128)(2,1)} %bitcast.18, bf16[512,2048]{1,0:T(8,128)(2,1)} %bitcast.57, bf16[2048,2816]{1,0:T(8,128)(2,1)} %all-gather.2.cloned.1.call-done, f32[512,1408]{1,0:T(8,128)} %fusion.14), kind=kOutput, calls=%fused_computation.31 | convolution fusion | flops 5910953984 | bytes 18612224 | tf_op jit(solution)/shard_map/dot_general | solution.py:163
  255.1 28.7 %reduce-scatter.2.cloned.1.call-done = bf16[128,2048]{1,0:T(8,128)(2,1)} async-done(((bf16[512,2048]{1,0:T(8,128)(2,1)}), bf16[128,2048]{1,0:T(8,128)(2,1)}) %reduce-scatter.2.cloned.1.call-update) | async-done | bytes 524304 | tf_op jit(solution)/shard_map/reduce_scatter | solution.py:162
  283.8 2.2 add_convert_fusion
  (25 shorter events, 0.2 us)
Async XLA Ops:
  6.5 22.5 %copy-start = (bf16[512,2048]{1,0:T(8,128)(2,1)S(1)}, bf16[512,2048]{1,0:T(8,128)(2,1)}, u32[]{:S(2)}) copy-start(bf16[512,2048]{1,0:T(8,128)(2,1)} %param.18) | copy-start | bytes 6291460
  6.5 107.2 %all-gather.2.cloned.1.call-start = ((), (), s32[]{:S(2)}) async-start(), calls=%async_computation.4 | async-start | bytes 11714560 | tf_op jit(solution)/shard_map/all_gather | solution.py:64
  9.2 7.1 %collective-permute-start.1 = (bf16[2,128,128]{2,1,0:T(8,128)(2,1)S(1)}, bf16[2,128,128]{2,1,0:T(8,128)(2,1)S(1)}, u32[]{:S(2)}, u32[]{:S(2)}) collective-permute-start(bf16[2,128,128]{2,1,0:T(8,128)(2,1)S(1)} %get-tuple-element.123), channel_id=1, source_target_pairs={{4,0},{8,4},{12,8},{16,12},{20,16},{24,20},{28,24},{32,28},{36,32}... | collective-permute-start | bytes 196616 | tf_op jit(solution)/shard_map/ppermute | solution.py:22
  14.3 3.2 %collective-permute-start = (bf16[2,128,128]{2,1,0:T(8,128)(2,1)S(1)}, bf16[2,128,128]{2,1,0:T(8,128)(2,1)S(1)}, u32[]{:S(2)}, u32[]{:S(2)}) collective-permute-start(bf16[2,128,128]{2,1,0:T(8,128)(2,1)S(1)} %get-tuple-element.122), channel_id=1, source_target_pairs={{0,4},{4,8},{8,12},{12,16},{16,20},{20,24},{24,28},{28,32},{32,36}... | collective-permute-start | bytes 196616 | tf_op jit(solution)/shard_map/ppermute | solution.py:20
  20.9 1.0 copy-start.3
  26.1 1.0 copy-start.3
  32.6 30.9 %all-to-all-start = ((bf16[4,128,2048]{2,1,0:T(8,128)(2,1)}), bf16[4,128,2048]{2,1,0:T(8,128)(2,1)}, u32[]{:S(2)}, u32[]{:S(2)}) async-start(bf16[4,128,2048]{2,1,0:T(8,128)(2,1)} %bitcast.55), calls=%async_computation | async-start | bytes 4194304 | tf_op jit(solution)/shard_map/all_to_all | solution.py:36
  37.0 29.3 %copy-start.4 = (f32[2048]{0:T(1024)S(1)}, f32[2048]{0:T(1024)}, u32[]{:S(2)}) copy-start(f32[2048]{0:T(1024)} %param.17) | copy-start | bytes 24580
  63.5 2.6 copy-start.1
  66.8 28.7 %copy-start.2 = (bf16[1408,32]{0,1:T(8,128)(2,1)S(1)}, bf16[1408,32]{0,1:T(8,128)(2,1)}, u32[]{:S(2)}) copy-start(bf16[1408,32]{0,1:T(8,128)(2,1)} %param.21) | copy-start | bytes 270340
  98.5 142.8 %all-to-all-start.2 = ((bf16[64,1408,32]{1,2,0:T(8,128)(2,1)}), bf16[64,1408,32]{1,2,0:T(8,128)(2,1)}, u32[]{:S(2)}, u32[]{:S(2)}) async-start(bf16[64,1408,32]{1,2,0:T(8,128)(2,1)} %stack.11), calls=%async_computation.2 | async-start | bytes 11534336 | tf_op jit(solution)/shard_map/all_to_all | solution.py:103
  113.5 170.4 %reduce-scatter.2.cloned.1.call-start = ((), (), s32[]{:S(2)}) async-start(), calls=%async_computation.5 | async-start | bytes 2621440 | tf_op jit(solution)/shard_map/reduce_scatter | solution.py:162
Sparse Core Ops, SparseCore 0:
  10.1 91.8 all-gather.1
  255.2 28.5 reduce-scatter.1
